TPU v7x, 32 devices: a whole 2x2x4 slice. The times are simulated.
32 devices in a mesh: kv: 8 (over z, x), tp: 4 (over y, core).
Axes of the slice: x: 2, y: 2, z: 4, core: 2. Of those that a mesh axis runs over, the one named last changes fastest.
Arguments:
- queries: bfloat16 [64, 4, 8, 128], P('kv', None, 'tp'), may hold values from -6 to 6
- keys: bfloat16 [64, 4, 8, 128], P('kv', None, 'tp'), may hold values from -6 to 6
- values: bfloat16 [64, 4, 8, 256], P('kv', None, 'tp'), may hold values from -6 to 6
- in_gate: float32 [64, 4, 8], P('kv', None, 'tp'), may hold values from -6 to 6
- forget_pre: float32 [64, 4, 8], P('kv', None, 'tp'), may hold values from -1 to 5
- old_keys: bfloat16 [64, 4, 8, 128], P('kv', None, 'tp'), may hold values from -6 to 6
- old_values: bfloat16 [64, 4, 8, 256], P('kv', None, 'tp'), may hold values from -6 to 6
- old_in_gate: float32 [64, 4, 8], P('kv', None, 'tp'), may hold values from -6 to 6
- old_forget: float32 [64, 4, 8], P('kv', None, 'tp'), may hold values from -1 to 5
- accepted: int32 [64], P('kv'), may hold values from 0 to 4
- state_mem: float32 [64, 8, 128, 256], P('kv', 'tp'), may hold values from -4 to 4
- state_norm: float32 [64, 8, 128], P('kv', 'tp'), may hold values from -6 to 6
- state_max: float32 [64, 8], P('kv', 'tp'), may hold values from -4 to 4
- norm_gain: float32 [8, 256], P('tp'), may hold values from 0.1 to 1.9
- out_weight: bfloat16 [2048, 2048], P('tp', 'kv'), may hold values from -0.125 to 0.125
Outputs:
- mixed: bfloat16 [64, 4, 2048], P('kv', 'tp')
- new_mem: float32 [64, 8, 128, 256], P('kv', 'tp')
- new_norm: float32 [64, 8, 128], P('kv', 'tp')
- new_max: float32 [64, 8], P('kv', 'tp')
Inputs may be any that keep to these rules, and one draw needn't show every extreme that they name: How many of the last step's 4 proposals of a sequence were accepted.
All inputs are finite; a program needn't handle non-finite values.
Results may differ from a plain program's by a relative error of at most 0.0068.
Values may be sent and summed in bfloat16 or wider, within the bound.
A program may use at most 64 MiB of HBM per device.

v0:
```python
import jax
import jax.numpy as jnp
from jax import lax
from jax.sharding import PartitionSpec as P

HIGH = lax.Precision.HIGHEST


def cell(queries, keys, values, in_gates, log_forget, memory, normal, stab):
    length = in_gates.shape[-1]
    causal = jnp.tril(jnp.ones((length, length), dtype=bool))
    cumul = jnp.cumsum(log_forget, axis=-1)
    logd = jnp.where(causal, cumul[:, :, None] - cumul[:, None, :] + in_gates[:, None, :], -jnp.inf)
    inter = cumul + stab[:, None]
    m_row = jnp.maximum(inter, jnp.max(logd, axis=-1))
    scores = jnp.einsum("hld,hsd->hls", queries, keys, precision=HIGH) * jnp.exp(
        logd - m_row[..., None]
    )
    w_inter = jnp.exp(inter - m_row)
    num = w_inter[..., None] * jnp.einsum(
        "hld,hde->hle", queries, memory, precision=HIGH
    ) + jnp.einsum("hls,hse->hle", scores, values, precision=HIGH)
    den = w_inter * jnp.einsum("hld,hd->hl", queries, normal, precision=HIGH) + jnp.sum(
        scores, axis=-1
    )
    hidden = num / jnp.maximum(jnp.abs(den), 1.0)[..., None]
    m_new = m_row[:, -1]
    g_state = jnp.exp(cumul[:, -1] + stab - m_new)
    g_tok = jnp.exp(cumul[:, -1:] - cumul + in_gates - m_new[:, None])
    mem_new = g_state[:, None, None] * memory + jnp.einsum(
        "hld,hle->hde", g_tok[..., None] * keys, values, precision=HIGH
    )
    norm_new = g_state[:, None] * normal + jnp.einsum("hl,hld->hd", g_tok, keys, precision=HIGH)
    return (hidden, mem_new, norm_new, m_new)


def one_sequence(
    queries,
    keys,
    values,
    in_gate,
    forget_pre,
    old_keys,
    old_values,
    old_in_gate,
    old_forget,
    accepted,
    memory,
    normal,
    stab,
    norm_gain,
):
    props = queries.shape[0]
    live = jnp.arange(props, dtype=jnp.int32) < accepted
    gates = jnp.concatenate([jnp.where(live[:, None], old_in_gate, -jnp.inf), in_gate], axis=0)
    forget = jnp.concatenate(
        [
            jnp.where(live[:, None], jax.nn.log_sigmoid(old_forget), 0.0),
            jax.nn.log_sigmoid(forget_pre),
        ],
        axis=0,
    )
    scale = queries.shape[-1] ** (-0.5)
    qrun = jnp.concatenate(
        [jnp.zeros(queries.shape, jnp.float32), queries.astype(jnp.float32) * scale], axis=0
    )
    krun = jnp.concatenate([old_keys, keys], axis=0).astype(jnp.float32)
    vrun = jnp.concatenate([old_values, values], axis=0).astype(jnp.float32)
    hidden, mem_new, norm_new, m_new = cell(
        jnp.swapaxes(qrun, 0, 1),
        jnp.swapaxes(krun, 0, 1),
        jnp.swapaxes(vrun, 0, 1),
        gates.T,
        forget.T,
        memory,
        normal,
        stab,
    )
    hidden = hidden[:, props:, :]
    mean = jnp.mean(hidden, -1, keepdims=True)
    var = jnp.mean(jnp.square(hidden - mean), -1, keepdims=True)
    normed = (hidden - mean) * lax.rsqrt(var + 1e-05) * norm_gain[:, None, :]
    flat = jnp.swapaxes(normed, 0, 1).reshape(props, -1).astype(jnp.bfloat16)
    return (flat, mem_new, norm_new, m_new)


def on_device(
    queries,
    keys,
    values,
    in_gate,
    forget_pre,
    old_keys,
    old_values,
    old_in_gate,
    old_forget,
    accepted,
    state_mem,
    state_norm,
    state_max,
    norm_gain,
    out_weight,
):
    mapped = jax.vmap(one_sequence, in_axes=(0, 0, 0, 0, 0, 0, 0, 0, 0, 0, 0, 0, 0, None))
    hidden, new_mem, new_norm, new_max = mapped(
        queries,
        keys,
        values,
        in_gate,
        forget_pre,
        old_keys,
        old_values,
        old_in_gate,
        old_forget,
        accepted,
        state_mem,
        state_norm,
        state_max,
        norm_gain,
    )
    terms = jnp.einsum(
        "spr,rc->spc",
        hidden,
        lax.all_gather(out_weight, "kv", axis=1, tiled=True),
        preferred_element_type=jnp.float32,
    )
    mixed = lax.psum_scatter(terms, "tp", scatter_dimension=1, tiled=True).astype(jnp.bfloat16)
    return (mixed, new_mem, new_norm, new_max)


def solution(mesh):
    return jax.shard_map(
        on_device,
        mesh=mesh,
        in_specs=(
            P("kv", None, "tp", None),
            P("kv", None, "tp", None),
            P("kv", None, "tp", None),
            P("kv", None, "tp"),
            P("kv", None, "tp"),
            P("kv", None, "tp", None),
            P("kv", None, "tp", None),
            P("kv", None, "tp"),
            P("kv", None, "tp"),
            P("kv"),
            P("kv", "tp", None, None),
            P("kv", "tp", None),
            P("kv", "tp"),
            P("tp", None),
            P("tp", "kv"),
        ),
        out_specs=(
            P("kv", "tp", None),
            P("kv", "tp", None, None),
            P("kv", "tp", None),
            P("kv", "tp"),
        ),
        check_vma=False,
    )
```

profile of v0, /device:TPU:0, one launch (start us, length us, event | category | flops | bytes accessed | tf_op | source)
XLA Modules:
  0.0 92.6 jit_solution(17613975096085614680)
XLA Ops:
  7.2 0.7 all-gather.2.cloned.1.call-update
  8.0 0.7 iota_compare_fusion.1
  8.6 0.7 fusion.19
  9.3 0.7 fusion.20
  10.1 0.7 copy.75
  10.9 0.1 copy.72
  10.9 0.1 fusion.5
  11.1 0.7 add_maximum_fusion
  11.8 0.1 copy.84
  11.9 0.7 copy.82
  12.7 0.7 copy.81
  13.4 0.7 convert_multiply_fusion
  14.1 0.2 fusion.27
  14.4 0.9 %fusion.7 = f32[8,2,1,8]{3,2,1,0:T(1,128)S(1)} fusion(f32[8,2,128,1]{2,3,1,0:T(1,128)} %bitcast.50, f32[8,2,8,128]{3,0,1,2:T(8,128)S(1)} %pad_bitcast_fusion), kind=kOutput, calls=%fused_computation.16 | convolution fusion | flops 196608 | bytes 74240 | tf_op jit(solution)/shard_map/vmap(hld,hd->hl)/dot_general | solution.py:23
  15.5 0.7 fusion.17
  16.2 0.1 copy.113
  16.3 0.8 copy.86
  17.0 0.8 copy.85
  17.8 0.1 copy.114
  17.9 0.3 fusion.11
  18.2 1.1 %fusion.9 = f32[8,2,8,256]{3,2,1,0:T(8,128)S(1)} fusion(f32[8,2,128,256]{3,2,1,0:T(8,128)S(1)} %copy-done, f32[8,2,8,128]{3,0,1,2:T(8,128)S(1)} %pad_bitcast_fusion), kind=kOutput, calls=%fused_computation.18 | convolution fusion | flops 50331648 | bytes 2293760 | tf_op jit(solution)/shard_map/vmap(hld,hde->hle)/dot_general | solution.py:20
  19.3 0.2 fusion.25
  19.5 0.2 multiply_reduce_fusion
  19.7 0.1 fusion.12
  19.9 0.1 copy.91
  20.2 0.2 fusion.14
  20.4 42.7 %all-gather.2.cloned.1.call-done = bf16[512,2048]{1,0:T(8,128)(2,1)} async-done(((bf16[512,256]{1,0:T(8,128)(2,1)}), bf16[512,2048]{1,0:T(8,128)(2,1)}) %all-gather.2.cloned.1.call-update) | async-done | bytes 2097168 | tf_op jit(solution)/shard_map/all_gather | solution.py:124
  63.1 2.8 %fusion = f32[8,4,2048]{2,0,1:T(8,128)} fusion(bf16[8,4,512]{2,0,1:T(8,128)(2,1)S(1)} %convert_element_type.20, bf16[512,2048]{1,0:T(8,128)(2,1)} %all-gather.2.cloned.1.call-done), kind=kOutput, calls=%fused_computation | convolution fusion | flops 67108864 | bytes 2392064 | tf_op jit(solution)/shard_map/spr,rc->spc/dot_general | solution.py:121
  65.9 0.7 multiply_add_fusion.1
  66.6 2.7 %multiply_add_fusion = f32[8,2,128,256]{3,2,1,0:T(8,128)} fusion(f32[8,2,128,256]{3,2,1,0:T(8,128)S(1)} %copy-done, f32[8,2]{1,0:T(8,128)S(1)} %copy.91, bf16[8,4,2,256]{3,1,2,0:T(4,128)(2,1)S(1)} %copy.86, bf16[8,4,2,256]{3,1,2,0:T(4,128)(2,1)S(1)} %copy.85, f32[8,2,8]{2,1,0:T(2,128)S(1)} %copy.92, bf16[8,4,2,128]{3,1,2,0:T(4,128)(2,1)S(1)} %copy.82, ...), kind=kOutput, calls=%fused_computation.2 | convolution fusion | flops 51609600 | bytes 4293184 | tf_op jit(solution)/shard_map/vmap(hld,hle->hde)/dot_general | solution.py:30
  69.3 15.0 %reduce-scatter.2.cloned.1.call-done = f32[8,1,2048]{2,0,1:T(8,128)} async-done(((f32[8,4,2048]{2,0,1:T(8,128)}), f32[8,1,2048]{2,0,1:T(8,128)}) %reduce-scatter.2.cloned.1.call-update) | async-done | bytes 65552 | tf_op jit(solution)/shard_map/reduce_scatter | solution.py:127
  84.3 1.5 %convert_element_type.21 = bf16[8,1,2048]{2,0,1:T(8,128)(2,1)} convert(f32[8,1,2048]{2,0,1:T(8,128)} %reduce-scatter.2.cloned.1.call-done) | non-fusion elementwise | flops 16384 | bytes 98304 | tf_op jit(solution)/shard_map/convert_element_type | solution.py:127
  (32 shorter events, 0.7 us)
Async XLA Ops:
  7.2 11.0 %copy-start = (f32[8,2,128,256]{3,2,1,0:T(8,128)S(1)}, f32[8,2,128,256]{3,2,1,0:T(8,128)}, u32[]{:S(2)}) copy-start(f32[8,2,128,256]{3,2,1,0:T(8,128)} %param.25) | copy-start | bytes 6291460
  7.2 55.9 %all-gather.2.cloned.1.call-start = ((), (), s32[]{:S(2)}) async-start(), calls=%async_computation.1 | async-start | bytes 2359296 | tf_op jit(solution)/shard_map/all_gather | solution.py:124
  7.9 76.4 %reduce-scatter.2.cloned.1.call-start = ((), (), s32[]{:S(2)}) async-start(), calls=%async_computation.2 | async-start | bytes 327680 | tf_op jit(solution)/shard_map/reduce_scatter | solution.py:127
  11.9 8.0 %copy-start.3 = (f32[8,2,1]{0,2,1:T(1,128)}, f32[8,2,1]{0,2,1:T(1,128)S(1)}, u32[]{:S(2)}) copy-start(f32[8,2,1]{0,2,1:T(1,128)S(1)} %slice.18) | copy-start | bytes 196
  14.1 5.6 %copy-start.4 = (f32[2,256]{1,0:T(2,128)S(1)}, f32[2,256]{1,0:T(2,128)}, u32[]{:S(2)}) copy-start(f32[2,256]{1,0:T(2,128)} %param.28) | copy-start | bytes 6148
  14.1 5.8 %copy-start.2 = (f32[8,2]{0,1:T(2,128)S(1)}, f32[8,2]{0,1:T(2,128)}, u32[]{:S(2)}) copy-start(f32[8,2]{0,1:T(2,128)} %param.27) | copy-start | bytes 196
  19.3 46.6 %copy-start.1 = (f32[8,2,128]{2,1,0:T(2,128)S(1)}, f32[8,2,128]{2,1,0:T(2,128)}, u32[]{:S(2)}) copy-start(f32[8,2,128]{2,1,0:T(2,128)} %param.26) | copy-start | bytes 24580
Sparse Core Ops, SparseCore 0:
  10.0 53.0 all-gather.1
  66.0 18.2 reduce-scatter.1
where the time goes:
time: 93.2 us; the launch traced here: 92.6 us
  waiting for transfers between devices  58.4 us (63%)
  between operations  14.2 us (15%)
  matrix products  8.2 us (9%)
  other arithmetic  6.98 us (7%)
  local copies, waits for them, and re-layouts  4.67 us (5%)
    all_gather x1, waiting for transfers between devices, on_device(): lax.all_gather(out_weight, 'kv', axis=1, tiled=True)  42.7 us
    reduce_scatter x1, waiting for transfers between devices, on_device(): lax.psum_scatter(terms, 'tp', scatter_dimension=1, tiled=True)  15 us
    unnamed x17, local copies, waits for them, and re-layouts  3.9 us
    dot_general x1, matrix products, on_device(): jnp.einsum('spr,rc->spc', hidden, lax.all_gather(out_weight, 'kv', axis=1...  2.77 us
    dot_general x1, matrix products, cell(): jnp.einsum('hld,hle->hde', g_tok[..., None] * keys, values, precision=HIGH)  2.7 us
  transfers between devices with their start and end apart: 2, of which 2 were waited for; matrix products, arithmetic and copies ran while one was open for 17% of the time, Pallas kernels for 0%

commit v1 on v0

--- a/solution.py
+++ b/solution.py
@@ -4,6 +4,25 @@
 from jax.sharding import PartitionSpec as P
 
 HIGH = lax.Precision.HIGHEST
+
+
+def in_order(tiles, dim):
+    tiles = jnp.moveaxis(tiles, 0, dim)
+    dims = tiles.shape
+    return tiles.reshape(*dims[:dim], dims[dim] * dims[dim + 1], *dims[dim + 2 :])
+
+
+def ring_apply(x, axis, dim, work, out_dim):
+    count, index, rows = (lax.axis_size(axis), lax.axis_index(axis), x.shape[dim])
+    right = [(i, (i + 1) % count) for i in range(count)]
+    tiles = []
+    held = x
+    for step in range(count):
+        coming = held if step == count - 1 else lax.ppermute(held, axis, right)
+        tiles.append(work(held, (index - step) % count * rows))
+        held = coming
+    tiles = jnp.stack(tiles)[(index - jnp.arange(count)) % count]
+    return in_order(tiles, out_dim)
 
 
 def cell(queries, keys, values, in_gates, log_forget, memory, normal, stab):
@@ -118,11 +137,14 @@
         state_max,
         norm_gain,
     )
-    terms = jnp.einsum(
-        "spr,rc->spc",
-        hidden,
-        lax.all_gather(out_weight, "kv", axis=1, tiled=True),
-        preferred_element_type=jnp.float32,
+    terms = ring_apply(
+        out_weight,
+        "kv",
+        1,
+        lambda shard, offset: jnp.einsum(
+            "spr,rc->spc", hidden, shard, preferred_element_type=jnp.float32
+        ),
+        2,
     )
     mixed = lax.psum_scatter(terms, "tp", scatter_dimension=1, tiled=True).astype(jnp.bfloat16)
     return (mixed, new_mem, new_norm, new_max)

time: 93.2 us -> 109 us (1.17)
  waiting for transfers between devices: 58.4 us -> 66.3 us
  starting transfers between devices: 0.08 us -> 4.67 us
  matrix products: 8.2 us -> 10.1 us
  local copies, waits for them, and re-layouts: 4.67 us -> 5.95 us
    ppermute x0 -> x7, waiting for transfers between devices: none -> 52.1 us  [ring_apply(): coming = held if step == count - 1 else lax.ppermute(held, axis, right)]
    all_gather x1 -> x0, waiting for transfers between devices: 42.7 us -> none  [on_device(): lax.all_gather(out_weight, 'kv', axis=1, tiled=True)]
    ppermute x0 -> x7, starting transfers between devices: none -> 4.63 us  [ring_apply(): coming = held if step == count - 1 else lax.ppermute(held, axis, right)]
    dot_general x1, matrix products: 1.11 us -> 2.69 us  [cell(): jnp.einsum('hld,hde->hle', queries, memory, precision=HIGH)]
    dot_general x1 -> x8, matrix products: 2.77 us -> 3.11 us  [on_device(): jnp.einsum('spr,rc->spc', hidden, shard, preferred_element_type=jnp.float32)]
    unnamed x17 -> x19, local copies, waits for them, and re-layouts: 3.9 us -> 3.9 us
  transfers between devices with their start and end apart: 2 -> 8, of which waited for: 2 -> 7; matrix products, arithmetic and copies ran while one was open for 17% -> 19% of each run, Pallas kernels for 0% -> 0%
where the time goes in v1:
time: 109 us; the launch traced here: 108 us
  waiting for transfers between devices  66.3 us (61%)
  between operations  14.3 us (13%)
  matrix products  10.1 us (9%)
  other arithmetic  7.01 us (6%)
  local copies, waits for them, and re-layouts  5.95 us (5%)
  starting transfers between devices  4.67 us (4%)
    ppermute x7, waiting for transfers between devices, ring_apply(): coming = held if step == count - 1 else lax.ppermute(held, axis, right)  52.1 us
    reduce_scatter x1, waiting for transfers between devices, on_device(): lax.psum_scatter(terms, 'tp', scatter_dimension=1, tiled=True)  14.1 us
    ppermute x7, starting transfers between devices, ring_apply(): coming = held if step == count - 1 else lax.ppermute(held, axis, right)  4.63 us
    unnamed x19, local copies, waits for them, and re-layouts  3.9 us
    dot_general x8, matrix products, on_device(): jnp.einsum('spr,rc->spc', hidden, shard, preferred_element_type=jnp.float32)  3.11 us
    dot_general x1, matrix products, cell(): jnp.einsum('hld,hde->hle', queries, memory, precision=HIGH)  2.69 us
    dot_general x1, matrix products, cell(): jnp.einsum('hld,hle->hde', g_tok[..., None] * keys, values, precision=HIGH)  2.69 us
  transfers between devices with their start and end apart: 8, of which 7 were waited for; matrix products, arithmetic and copies ran while one was open for 19% of the time, Pallas kernels for 0%

profile of v1, /device:TPU:0, one launch (start us, length us, event | category | flops | bytes accessed | tf_op | source)
XLA Modules:
  0.0 108.3 jit_solution(4853809156253745034)
XLA Ops:
  7.2 3.0 %collective-permute-start = (bf16[512,256]{1,0:T(8,128)(2,1)}, bf16[512,256]{1,0:T(8,128)(2,1)S(1)}, u32[]{:S(2)}, u32[]{:S(2)}) collective-permute-start(bf16[512,256]{1,0:T(8,128)(2,1)} %param.29), channel_id=1, source_target_pairs={{0,4},{4,8},{8,12},{12,16},{16,20},{20,24},{24,28},{28,0},{1,5},{5... | collective-permute-start | bytes 786440 | tf_op jit(solution)/shard_map/ppermute | solution.py:21
  10.2 0.7 iota_compare_fusion.1
  10.9 0.7 copy.77
  11.6 0.7 fusion.34
  12.3 0.7 fusion.33
  13.4 0.7 add_maximum_fusion
  14.2 0.7 copy.84
  14.9 0.7 copy.83
  15.7 0.8 copy.88
  16.4 0.8 copy.87
  17.2 0.7 convert_multiply_fusion
  18.0 1.0 fusion.21
  19.0 0.2 fusion.43
  19.3 0.7 fusion.31
  20.3 0.2 fusion.28
  20.5 2.7 %fusion.23 = f32[8,2,8,256]{3,2,1,0:T(8,128)S(1)} fusion(f32[8,2,128,256]{3,2,1,0:T(8,128)} %param.25, f32[8,2,8,128]{3,0,1,2:T(8,128)S(1)} %pad_bitcast_fusion), kind=kOutput, calls=%fused_computation.41 | convolution fusion | flops 50331648 | bytes 2293760 | tf_op jit(solution)/shard_map/vmap(hld,hde->hle)/dot_general | solution.py:39
  23.2 0.3 fusion.25
  23.7 1.6 %collective-permute-start.1 = (bf16[512,256]{1,0:T(8,128)(2,1)S(1)}, bf16[512,256]{1,0:T(8,128)(2,1)S(1)}, u32[]{:S(2)}, u32[]{:S(2)}) collective-permute-start(bf16[512,256]{1,0:T(8,128)(2,1)S(1)} %collective-permute-done), channel_id=1, source_target_pairs={{0,4},{4,8},{8,12},{12,16},{16,20},{20,24},{24,28},{28,0},{1,5},{5... | collective-permute-start | bytes 786440 | tf_op jit(solution)/shard_map/ppermute | solution.py:21
  25.5 8.7 %collective-permute-done.1 = bf16[512,256]{1,0:T(8,128)(2,1)S(1)} collective-permute-done((bf16[512,256]{1,0:T(8,128)(2,1)S(1)}, bf16[512,256]{1,0:T(8,128)(2,1)S(1)}, u32[]{:S(2)}, u32[]{:S(2)}) %collective-permute-start.1) | collective-permute-done | bytes 262176 | tf_op jit(solution)/shard_map/ppermute | solution.py:21
  34.4 9.5 %collective-permute-done.2 = bf16[512,256]{1,0:T(8,128)(2,1)} collective-permute-done((bf16[512,256]{1,0:T(8,128)(2,1)S(1)}, bf16[512,256]{1,0:T(8,128)(2,1)}, u32[]{:S(2)}, u32[]{:S(2)}) %collective-permute-start.2) | collective-permute-done | bytes 262176 | tf_op jit(solution)/shard_map/ppermute | solution.py:21
  44.3 9.0 %collective-permute-done.3 = bf16[512,256]{1,0:T(8,128)(2,1)} collective-permute-done((bf16[512,256]{1,0:T(8,128)(2,1)}, bf16[512,256]{1,0:T(8,128)(2,1)}, u32[]{:S(2)}, u32[]{:S(2)}) %collective-permute-start.3) | collective-permute-done | bytes 262176 | tf_op jit(solution)/shard_map/ppermute | solution.py:21
  53.6 9.0 %collective-permute-done.4 = bf16[512,256]{1,0:T(8,128)(2,1)S(1)} collective-permute-done((bf16[512,256]{1,0:T(8,128)(2,1)}, bf16[512,256]{1,0:T(8,128)(2,1)S(1)}, u32[]{:S(2)}, u32[]{:S(2)}) %collective-permute-start.4) | collective-permute-done | bytes 262176 | tf_op jit(solution)/shard_map/ppermute | solution.py:21
  62.6 1.1 %fusion.4 = f32[8,8,4,256]{3,1,2,0:T(8,128)S(1)} fusion(f32[8,8,4,256]{3,1,2,0:T(8,128)S(1)} %fusion.5, bf16[8,4,512]{2,0,1:T(8,128)(2,1)S(1)} %convert_element_type.20, bf16[512,256]{1,0:T(8,128)(2,1)} %collective-permute-done.2), kind=kOutput, calls=%fused_computation.12 | convolution fusion | flops 8388608 | bytes 327680 | tf_op jit(solution)/shard_map/spr,rc->spc/dot_general | solution.py:144
  63.7 1.1 %fusion.3 = f32[8,8,4,256]{3,1,2,0:T(8,128)S(1)} fusion(f32[8,8,4,256]{3,1,2,0:T(8,128)S(1)} %fusion.4, bf16[8,4,512]{2,0,1:T(8,128)(2,1)S(1)} %convert_element_type.20, bf16[512,256]{1,0:T(8,128)(2,1)} %collective-permute-done.3), kind=kOutput, calls=%fused_computation.10 | convolution fusion | flops 8388608 | bytes 327680 | tf_op jit(solution)/shard_map/spr,rc->spc/dot_general | solution.py:144
  64.8 7.2 %collective-permute-done.5 = bf16[512,256]{1,0:T(8,128)(2,1)S(1)} collective-permute-done((bf16[512,256]{1,0:T(8,128)(2,1)S(1)}, bf16[512,256]{1,0:T(8,128)(2,1)S(1)}, u32[]{:S(2)}, u32[]{:S(2)}) %collective-permute-start.5) | collective-permute-done | bytes 262176 | tf_op jit(solution)/shard_map/ppermute | solution.py:21
  72.3 8.8 %collective-permute-done.6 = bf16[512,256]{1,0:T(8,128)(2,1)S(1)} collective-permute-done((bf16[512,256]{1,0:T(8,128)(2,1)S(1)}, bf16[512,256]{1,0:T(8,128)(2,1)S(1)}, u32[]{:S(2)}, u32[]{:S(2)}) %collective-permute-start.6) | collective-permute-done | bytes 262176 | tf_op jit(solution)/shard_map/ppermute | solution.py:21
  81.2 0.6 gather_fusion
  81.8 0.7 copy.102
  82.5 0.7 multiply_add_fusion.1
  83.2 2.7 %multiply_add_fusion = f32[8,2,128,256]{3,2,1,0:T(8,128)} fusion(f32[8,2,128,256]{3,2,1,0:T(8,128)S(1)} %copy-done, f32[8,2]{1,0:T(8,128)S(1)} %copy.94, bf16[8,4,2,256]{3,1,2,0:T(4,128)(2,1)S(1)} %copy.88, bf16[8,4,2,256]{3,1,2,0:T(4,128)(2,1)S(1)} %copy.87, f32[8,2,8]{2,1,0:T(2,128)S(1)} %copy.95, bf16[8,4,2,128]{3,1,2,0:T(4,128)(2,1)S(1)} %copy.84, ...), kind=kOutput, calls=%fused_computation.1 | convolution fusion | flops 51609600 | bytes 4293184 | tf_op jit(solution)/shard_map/vmap(hld,hle->hde)/dot_general | solution.py:49
  85.9 14.1 %reduce-scatter.2.cloned.1.call-done = f32[8,1,2048]{2,0,1:T(8,128)} async-done(((f32[8,4,2048]{2,0,1:T(8,128)}), f32[8,1,2048]{2,0,1:T(8,128)}) %reduce-scatter.2.cloned.1.call-update) | async-done | bytes 65552 | tf_op jit(solution)/shard_map/reduce_scatter | solution.py:149
  100.0 1.5 %convert_element_type.21 = bf16[8,1,2048]{2,0,1:T(8,128)(2,1)} convert(f32[8,1,2048]{2,0,1:T(8,128)} %reduce-scatter.2.cloned.1.call-done) | non-fusion elementwise | flops 16384 | bytes 98304 | tf_op jit(solution)/shard_map/convert_element_type | solution.py:149
  (56 shorter events, 2.6 us)
Async XLA Ops:
  7.2 92.8 %reduce-scatter.2.cloned.1.call-start = ((), (), s32[]{:S(2)}) async-start(), calls=%async_computation.1 | async-start | bytes 327680 | tf_op jit(solution)/shard_map/reduce_scatter | solution.py:149
  7.2 16.5 %collective-permute-start = (bf16[512,256]{1,0:T(8,128)(2,1)}, bf16[512,256]{1,0:T(8,128)(2,1)S(1)}, u32[]{:S(2)}, u32[]{:S(2)}) collective-permute-start(bf16[512,256]{1,0:T(8,128)(2,1)} %param.29), channel_id=1, source_target_pairs={{0,4},{4,8},{8,12},{12,16},{16,20},{20,24},{24,28},{28,0},{1,5},{5... | collective-permute-start | bytes 786440 | tf_op jit(solution)/shard_map/ppermute | solution.py:21
  14.1 9.5 %copy-start.4 = (f32[8,2,1]{0,2,1:T(1,128)}, f32[8,2,1]{0,2,1:T(1,128)S(1)}, u32[]{:S(2)}) copy-start(f32[8,2,1]{0,2,1:T(1,128)S(1)} %slice.20) | copy-start | bytes 196
  17.9 5.7 %copy-start.3 = (f32[8,2]{0,1:T(2,128)S(1)}, f32[8,2]{0,1:T(2,128)}, u32[]{:S(2)}) copy-start(f32[8,2]{0,1:T(2,128)} %param.27) | copy-start | bytes 196
  17.9 16.3 %copy-start.5 = (f32[2,256]{1,0:T(2,128)S(1)}, f32[2,256]{1,0:T(2,128)}, u32[]{:S(2)}) copy-start(f32[2,256]{1,0:T(2,128)} %param.28) | copy-start | bytes 6148
  19.0 25.2 %copy-start.1 = (bf16[512,256]{1,0:T(8,128)(2,1)S(1)}, bf16[512,256]{1,0:T(8,128)(2,1)}, u32[]{:S(2)}) copy-start(bf16[512,256]{1,0:T(8,128)(2,1)} %param.29) | copy-start | bytes 786436
  23.7 10.5 %collective-permute-start.1 = (bf16[512,256]{1,0:T(8,128)(2,1)S(1)}, bf16[512,256]{1,0:T(8,128)(2,1)S(1)}, u32[]{:S(2)}, u32[]{:S(2)}) collective-permute-start(bf16[512,256]{1,0:T(8,128)(2,1)S(1)} %collective-permute-done), channel_id=1, source_target_pairs={{0,4},{4,8},{8,12},{12,16},{16,20},{20,24},{24,28},{28,0},{1,5},{5... | collective-permute-start | bytes 786440 | tf_op jit(solution)/shard_map/ppermute | solution.py:21
  34.2 9.7 %collective-permute-start.2 = (bf16[512,256]{1,0:T(8,128)(2,1)S(1)}, bf16[512,256]{1,0:T(8,128)(2,1)}, u32[]{:S(2)}, u32[]{:S(2)}) collective-permute-start(bf16[512,256]{1,0:T(8,128)(2,1)S(1)} %collective-permute-done.1), channel_id=1, source_target_pairs={{0,4},{4,8},{8,12},{12,16},{16,20},{20,24},{24,28},{28,0},{1,5},{5... | collective-permute-start | bytes 786440 | tf_op jit(solution)/shard_map/ppermute | solution.py:21
  34.2 48.3 %copy-start.2 = (f32[8,2,128]{2,1,0:T(2,128)S(1)}, f32[8,2,128]{2,1,0:T(2,128)}, u32[]{:S(2)}) copy-start(f32[8,2,128]{2,1,0:T(2,128)} %param.26) | copy-start | bytes 24580
  34.3 48.9 %copy-start = (f32[8,2,128,256]{3,2,1,0:T(8,128)S(1)}, f32[8,2,128,256]{3,2,1,0:T(8,128)}, u32[]{:S(2)}) copy-start(f32[8,2,128,256]{3,2,1,0:T(8,128)} %param.25) | copy-start | bytes 6291460
  43.9 9.4 %collective-permute-start.3 = (bf16[512,256]{1,0:T(8,128)(2,1)}, bf16[512,256]{1,0:T(8,128)(2,1)}, u32[]{:S(2)}, u32[]{:S(2)}) collective-permute-start(bf16[512,256]{1,0:T(8,128)(2,1)} %collective-permute-done.2), channel_id=1, source_target_pairs={{0,4},{4,8},{8,12},{12,16},{16,20},{20,24},{24,28},{28,0},{1,5},{5... | collective-permute-start | bytes 786440 | tf_op jit(solution)/shard_map/ppermute | solution.py:21
  53.3 9.3 %collective-permute-start.4 = (bf16[512,256]{1,0:T(8,128)(2,1)}, bf16[512,256]{1,0:T(8,128)(2,1)S(1)}, u32[]{:S(2)}, u32[]{:S(2)}) collective-permute-start(bf16[512,256]{1,0:T(8,128)(2,1)} %collective-permute-done.3), channel_id=1, source_target_pairs={{0,4},{4,8},{8,12},{12,16},{16,20},{20,24},{24,28},{28,0},{1,5},{5... | collective-permute-start | bytes 786440 | tf_op jit(solution)/shard_map/ppermute | solution.py:21
  62.6 9.4 %collective-permute-start.5 = (bf16[512,256]{1,0:T(8,128)(2,1)S(1)}, bf16[512,256]{1,0:T(8,128)(2,1)S(1)}, u32[]{:S(2)}, u32[]{:S(2)}) collective-permute-start(bf16[512,256]{1,0:T(8,128)(2,1)S(1)} %collective-permute-done.4), channel_id=1, source_target_pairs={{0,4},{4,8},{8,12},{12,16},{16,20},{20,24},{24,28},{28,0},{1,5},{5... | collective-permute-start | bytes 786440 | tf_op jit(solution)/shard_map/ppermute | solution.py:21
  72.0 9.1 %collective-permute-start.6 = (bf16[512,256]{1,0:T(8,128)(2,1)S(1)}, bf16[512,256]{1,0:T(8,128)(2,1)S(1)}, u32[]{:S(2)}, u32[]{:S(2)}) collective-permute-start(bf16[512,256]{1,0:T(8,128)(2,1)S(1)} %collective-permute-done.5), channel_id=1, source_target_pairs={{0,4},{4,8},{8,12},{12,16},{16,20},{20,24},{24,28},{28,0},{1,5},{5... | collective-permute-start | bytes 786440 | tf_op jit(solution)/shard_map/ppermute | solution.py:21
Sparse Core Ops, SparseCore 0:
  82.6 17.3 reduce-scatter.1
